TPU v7x, 32 devices: a whole 2x2x4 slice. The times are simulated.
32 devices in a mesh: gr: 2 (over core), fs: 8 (over z, y), tp: 2 (over x).
Axes of the slice: x: 2, y: 2, z: 4, core: 2. Of those that a mesh axis runs over, the one named last changes fastest.
Arguments:
- tokens: bfloat16 [3072, 2048], P(('gr', 'fs')), may hold values from -6 to 6
- routes: int32 [3072, 8], P(('gr', 'fs')), may hold values from 0 to 15, all different within a row; in each aligned block of 192 rows (0 to 191, 192 to 383, ...) at most 144 rows name the same one
- route_weight: float32 [3072, 8], P(('gr', 'fs')), may hold values from 0.05 to 0.6
- norm_gain: float32 [2048], replicated, may hold values from 0.1 to 1.9
- gate_experts: float32 [2, 8, 512, 2048], P('gr', None, 'fs', 'tp'), may hold values from -0.125 to 0.125
- up_experts: float32 [2, 8, 512, 2048], P('gr', None, 'fs', 'tp'), may hold values from -0.125 to 0.125
- down_experts: float32 [2, 8, 512, 2048], P('gr', None, 'fs', 'tp'), may hold values from -0.25 to 0.25
- gate_shared: float32 [2048, 512], P('fs', 'tp'), may hold values from -0.125 to 0.125
- up_shared: float32 [2048, 512], P('fs', 'tp'), may hold values from -0.125 to 0.125
- down_shared: float32 [512, 2048], P('fs', 'tp'), may hold values from -0.25 to 0.25
Outputs:
- mixed: bfloat16 [3072, 2048], P(('gr', 'fs'), 'tp')
- gate_served: bfloat16 [2, 8, 512, 2048], P(None, 'fs', 'tp')
- up_served: bfloat16 [2, 8, 512, 2048], P(None, 'fs', 'tp')
- down_served: bfloat16 [2, 8, 512, 2048], P(None, 'fs', None, 'tp')
- gate_shared_served: bfloat16 [2048, 512], P(None, 'tp')
- up_shared_served: bfloat16 [2048, 512], P(None, 'tp')
- down_shared_served: bfloat16 [512, 2048], P(None, 'tp')
Inputs may be any that keep to these rules, and one draw needn't show every extreme that they name: `routes`: each row names 8 different experts; within the 192 rows of one device no expert is named by more than 144 rows, and some expert reaches 144.
All inputs are finite; a program needn't handle non-finite values.
Results may differ from a plain program's by a relative error of at most 0.0084.
Values may be sent and summed in bfloat16 or wider, within the bound.
A program may use at most 128 MiB of HBM per device.

v0:
```python
import jax
import jax.numpy as jnp
from jax import lax
from jax.sharding import PartitionSpec as P

EXP_HALF = 1
EPS = 1e-06


def on_device(
    tokens,
    routes,
    route_weight,
    norm_gain,
    gate_experts,
    up_experts,
    down_experts,
    gate_shared,
    up_shared,
    down_shared,
):
    bf = jnp.bfloat16
    f32 = jnp.float32
    n_fs = lax.axis_size("fs")
    n_gr = lax.axis_size("gr")
    n_tp = lax.axis_size("tp")
    fs_index = lax.axis_index("fs")
    cols_here = gate_experts.shape[3]
    gain_cols = lax.dynamic_slice_in_dim(norm_gain, lax.axis_index("tp") * cols_here, cols_here, 0)
    gate_local = (gate_experts * gain_cols[None, None, None, :]).astype(bf)
    up_local = (up_experts * gain_cols[None, None, None, :]).astype(bf)
    down_local = down_experts.astype(bf)
    shared_here = gate_shared.shape[0]
    gain_shared = lax.dynamic_slice_in_dim(norm_gain, fs_index * shared_here, shared_here, 0)
    gate_sh_local = (gate_shared * gain_shared[:, None]).astype(bf)
    up_sh_local = (up_shared * gain_shared[:, None]).astype(bf)
    down_sh_local = down_shared.astype(bf)
    halves = (
        lax.all_gather(gate_local, "gr", axis=0, tiled=True),
        lax.all_gather(up_local, "gr", axis=0, tiled=True),
        lax.all_gather(down_local, "gr", axis=0, tiled=True),
    )
    gate_cols, up_cols, down_w = (
        lax.all_to_all(halves[0], "fs", split_axis=1, concat_axis=2, tiled=True),
        lax.all_to_all(halves[1], "fs", split_axis=1, concat_axis=2, tiled=True),
        lax.all_to_all(halves[2], "fs", split_axis=1, concat_axis=2, tiled=True),
    )
    gate_w, up_w = (
        lax.all_to_all(gate_cols, "tp", split_axis=2, concat_axis=3, tiled=True),
        lax.all_to_all(up_cols, "tp", split_axis=2, concat_axis=3, tiled=True),
    )
    gate_sw, up_sw, down_sw = (
        lax.all_gather(gate_sh_local, "fs", axis=0, tiled=True),
        lax.all_gather(up_sh_local, "fs", axis=0, tiled=True),
        lax.all_gather(down_sh_local, "fs", axis=0, tiled=True),
    )
    values = tokens.astype(f32)
    normed = (values * lax.rsqrt(jnp.mean(values * values, axis=-1, keepdims=True) + EPS)).astype(
        bf
    )
    tok_count, top = routes.shape
    width = tokens.shape[1]
    per_group = gate_experts.shape[1]
    count = per_group * n_gr
    capacity = (3 * tok_count * top + 2 * count - 1) // (2 * count)
    flat_e = routes.reshape(-1)
    onehot = (flat_e[:, None] == jnp.arange(count, dtype=jnp.int32)[None, :]).astype(jnp.int32)
    ranks = jnp.sum(jnp.cumsum(onehot, axis=0) * onehot, axis=1) - 1
    group_of = flat_e // per_group
    within = flat_e % per_group
    target = within // EXP_HALF
    local_k = within % EXP_HALF
    slot = ((target * n_gr + group_of) * EXP_HALF + local_k) * capacity + ranks
    total_slots = n_fs * n_gr * EXP_HALF * capacity
    repeated = jnp.repeat(normed, top, axis=0)
    send = jnp.zeros((total_slots, width), bf).at[slot].set(repeated)
    send = send.reshape(n_fs, n_gr, EXP_HALF, capacity, width)
    cols = width // n_tp
    send = lax.dynamic_slice_in_dim(send, lax.axis_index("tp") * cols, cols, 4)
    received = lax.all_to_all(send, "fs", split_axis=0, concat_axis=0, tiled=True)
    received = lax.all_gather(received, "tp", axis=4, tiled=True)
    gate = jnp.einsum("sgkcd,gkfd->sgkcf", received, gate_w, preferred_element_type=f32)
    upper = jnp.einsum("sgkcd,gkfd->sgkcf", received, up_w, preferred_element_type=f32)
    hidden = (jax.nn.silu(gate) * upper).astype(bf)
    full_hidden = lax.all_gather(hidden, "tp", axis=4, tiled=True)
    result = jnp.einsum(
        "sgkcf,gkfe->sgkce", full_hidden, down_w, preferred_element_type=f32
    ).astype(bf)
    returned = lax.all_to_all(result, "fs", split_axis=0, concat_axis=0, tiled=True)
    picked = returned.reshape(total_slots, cols)[slot].reshape(tok_count, top, cols)
    routed = jnp.einsum("tkc,tk->tc", picked.astype(f32), route_weight)
    shared_gate = jnp.dot(normed, gate_sw, preferred_element_type=f32)
    shared_up = jnp.dot(normed, up_sw, preferred_element_type=f32)
    shared_hidden = (jax.nn.silu(shared_gate) * shared_up).astype(bf)
    shared_full = lax.all_gather(shared_hidden, "tp", axis=1, tiled=True)
    shared = jnp.dot(shared_full, down_sw, preferred_element_type=f32)
    mixed = (routed + shared).astype(bf)
    return (mixed, gate_w, up_w, down_w, gate_sw, up_sw, down_sw)


def solution(mesh):
    return jax.shard_map(
        on_device,
        mesh=mesh,
        in_specs=(
            P(("gr", "fs"), None),
            P(("gr", "fs"), None),
            P(("gr", "fs"), None),
            P(),
            P("gr", None, "fs", "tp"),
            P("gr", None, "fs", "tp"),
            P("gr", None, "fs", "tp"),
            P("fs", "tp"),
            P("fs", "tp"),
            P("fs", "tp"),
        ),
        out_specs=(
            P(("gr", "fs"), "tp"),
            P(None, "fs", "tp", None),
            P(None, "fs", "tp", None),
            P(None, "fs", None, "tp"),
            P(None, "tp"),
            P(None, "tp"),
            P(None, "tp"),
        ),
        check_vma=False,
    )
```

profile of v0, /device:TPU:0, one launch (start us, length us, event | category | flops | bytes accessed | tf_op | source)
XLA Modules:
  0.0 651.1 jit_solution(783318843968911715)
XLA Ops:
  8.0 0.9 copy.58
  9.2 4.5 reduce-window.6
  14.6 1.4 fusion.21
  16.2 14.7 %scatter_custom_fusion = bf16[2304,2048]{1,0:T(8,128)(2,1)} fusion(s32[1536]{0:T(1024)S(1)} %fusion.28, bf16[]{:T(256)} %constant.72.clone.1, bf16[192,2048]{1,0:T(8,128)(2,1)S(1)} %fusion.22), kind=kCustom, calls=%fused_computation.6 | custom fusion | bytes 10223618 | tf_op jit(solution)/shard_map/scatter | solution.py:76
  30.9 5.3 dynamic-slice_bitcast_fusion
  36.2 7.4 %all-to-all-start.2 = ((bf16[8,2,1,144,1024]{4,3,1,2,0:T(8,128)(2,1)}), bf16[8,2,1,144,1024]{4,3,1,2,0:T(8,128)(2,1)}, u32[]{:S(2)}, u32[]{:S(2)}) async-start(bf16[8,2,1,144,1024]{4,3,1,2,0:T(8,128)(2,1)} %dynamic-slice_bitcast_fusion), calls=%async_computation.2 | async-start | bytes 9437184 | tf_op jit(solution)/shard_map/all_to_all | solution.py:80
  43.7 3.5 multiply_convert_fusion.1
  47.3 0.7 all-gather.9.cloned.1.call-update
  48.0 0.8 copy-done.6
  48.8 1.1 convert_element_type.57
  49.9 9.4 %all-gather.13.cloned.1.call-done = bf16[2,8,64,1024]{3,2,1,0:T(8,128)(2,1)} async-done(((bf16[1,8,64,1024]{3,2,1,0:T(8,128)(2,1)}), bf16[2,8,64,1024]{3,2,1,0:T(8,128)(2,1)}) %all-gather.13.cloned.1.call-update) | async-done | bytes 2097168 | tf_op jit(solution)/shard_map/all_gather | solution.py:40
  59.3 3.1 copy.63
  62.4 85.7 %all-to-all-done.2 = bf16[8,2,1,144,1024]{4,3,1,2,0:T(8,128)(2,1)} async-done(((bf16[8,2,1,144,1024]{4,3,1,2,0:T(8,128)(2,1)}), bf16[8,2,1,144,1024]{4,3,1,2,0:T(8,128)(2,1)}, u32[]{:S(2)}, u32[]{:S(2)}) %all-to-all-start.2) | async-done | bytes 4718624 | tf_op jit(solution)/shard_map/all_to_all | solution.py:80
  148.2 3.6 all-to-all-start.3
  151.8 0.5 all-gather.11.cloned.1.call-start
  152.3 5.3 copy.62
  157.6 3.1 copy.53
  160.8 39.5 %all-to-all-done.3 = bf16[2,8,64,1024]{3,2,0,1:T(8,128)(2,1)S(1)} async-done(((bf16[2,8,64,1024]{3,2,0,1:T(8,128)(2,1)}), bf16[2,8,64,1024]{3,2,0,1:T(8,128)(2,1)S(1)}, u32[]{:S(2)}, u32[]{:S(2)}) %all-to-all-start.3) | async-done | bytes 2097184 | tf_op jit(solution)/shard_map/all_to_all | solution.py:45
  200.2 4.4 all-to-all-start
  204.8 3.5 copy.65
  208.2 44.2 %all-to-all-done = bf16[2,8,64,1024]{3,2,0,1:T(8,128)(2,1)} async-done(((bf16[2,8,64,1024]{3,2,0,1:T(8,128)(2,1)}), bf16[2,8,64,1024]{3,2,0,1:T(8,128)(2,1)}, u32[]{:S(2)}, u32[]{:S(2)}) %all-to-all-start) | async-done | bytes 2097184 | tf_op jit(solution)/shard_map/all_to_all | solution.py:44
  252.4 3.8 all-to-all-start.4
  256.2 1.8 copy.54
  257.9 3.5 copy.55
  261.4 37.9 %all-to-all-done.4 = bf16[2,1,512,1024]{3,0,1,2:T(2,128)(2,1)S(1)} async-done(((bf16[2,1,512,1024]{3,0,1,2:T(2,128)(2,1)}), bf16[2,1,512,1024]{3,0,1,2:T(2,128)(2,1)S(1)}, u32[]{:S(2)}, u32[]{:S(2)}) %all-to-all-start.4) | async-done | bytes 2097184 | tf_op jit(solution)/shard_map/all_to_all | solution.py:50
  299.3 4.8 all-to-all-start.1
  304.2 3.1 copy.68
  307.3 2.2 copy.66
  309.5 3.5 copy.67
  313.0 4.5 reshape.245
  317.5 11.3 %all-to-all-done.1 = bf16[2,1,512,1024]{3,0,1,2:T(2,128)(2,1)} async-done(((bf16[2,1,512,1024]{3,0,1,2:T(2,128)(2,1)}), bf16[2,1,512,1024]{3,0,1,2:T(2,128)(2,1)}, u32[]{:S(2)}, u32[]{:S(2)}) %all-to-all-start.1) | async-done | bytes 2097184 | tf_op jit(solution)/shard_map/all_to_all | solution.py:49
  328.8 6.1 all-to-all-start.5
  335.1 2.2 copy.56
  337.3 1.3 copy-done
  338.6 3.5 copy.57
  342.1 4.5 reshape.244
  346.6 6.0 fusion
  352.6 1.6 copy-done.14
  354.2 4.1 fusion.10
  358.4 24.0 %all-to-all-done.5 = bf16[2,8,64,1024]{3,2,0,1:T(8,128)(2,1)} async-done(((bf16[2,8,64,1024]{3,2,0,1:T(8,128)(2,1)}), bf16[2,8,64,1024]{3,2,0,1:T(8,128)(2,1)}, u32[]{:S(2)}, u32[]{:S(2)}) %all-to-all-start.5) | async-done | bytes 2097184 | tf_op jit(solution)/shard_map/all_to_all | solution.py:46
  382.4 3.1 copy.69
  385.5 9.5 %all-gather.15.cloned.1.call-done = bf16[8,2,1,144,512]{4,3,0,1,2:T(8,128)(2,1)} async-done(((bf16[8,2,1,144,256]{4,3,0,1,2:T(8,128)(2,1)}), bf16[8,2,1,144,512]{4,3,0,1,2:T(8,128)(2,1)}) %all-gather.15.cloned.1.call-update) | async-done | bytes 2359312 | tf_op jit(solution)/shard_map/all_gather | solution.py:85
  395.0 4.9 convert_bitcast_fusion
  399.9 2.7 copy.70
  402.6 5.7 all-to-all-start.6
  408.5 1.8 multiply_convert_fusion.3
  410.3 0.5 all-gather.21.cloned.1.call-update
  410.9 0.7 convert_element_type.65
  411.8 114.1 %all-gather.19.cloned.1.call-done = bf16[2048,256]{1,0:T(8,128)(2,1)} async-done(((bf16[256,256]{1,0:T(8,128)(2,1)}), bf16[2048,256]{1,0:T(8,128)(2,1)}) %all-gather.19.cloned.1.call-update) | async-done | bytes 1048592 | tf_op jit(solution)/shard_map/all_gather | solution.py:53
  525.8 39.1 %all-gather.21.cloned.1.call-done = bf16[2048,256]{1,0:T(8,128)(2,1)} async-done(((bf16[256,256]{1,0:T(8,128)(2,1)}), bf16[2048,256]{1,0:T(8,128)(2,1)}) %all-gather.21.cloned.1.call-update) | async-done | bytes 1048592 | tf_op jit(solution)/shard_map/all_gather | solution.py:54
  565.0 41.5 %all-gather.23.cloned.1.call-done = bf16[512,1024]{1,0:T(8,128)(2,1)} async-done(((bf16[64,1024]{1,0:T(8,128)(2,1)}), bf16[512,1024]{1,0:T(8,128)(2,1)}) %all-gather.23.cloned.1.call-update) | async-done | bytes 1048592 | tf_op jit(solution)/shard_map/all_gather | solution.py:55
  606.5 1.6 fusion.31
  608.1 1.6 fusion.24
  609.7 5.5 all_gather.34
  615.2 3.9 copy.71
  619.2 2.6 copy.72
  621.7 4.1 copy.74
  625.8 2.4 copy.75
  628.2 10.0 %gather_fusion = bf16[1536,1024]{1,0:T(8,128)(2,1)S(1)} fusion(bf16[2304,1024]{1,0:T(8,128)(2,1)} %bitcast.25, s32[2048]{0:T(1024)S(1)} %pad_clamp_fusion), kind=kCustom, calls=%fused_computation | custom fusion | bytes 6297600 | tf_op jit(solution)/shard_map/gather | solution.py:90
  638.3 1.0 fusion.7
  639.5 1.1 fusion.23
  640.6 1.0 copy.88
  641.6 1.0 copy.89
  642.6 1.0 copy.90
  (62 shorter events, 2.7 us)
Async XLA Ops:
  8.0 8.0 %copy-start.5 = (bf16[192,2048]{1,0:T(8,128)(2,1)S(1)}, bf16[192,2048]{1,0:T(8,128)(2,1)}, u32[]{:S(2)}) copy-start(bf16[192,2048]{1,0:T(8,128)(2,1)} %param.10) | copy-start | bytes 2359300
  36.2 7.5 %copy-start.8 = (f32[1,8,64,1024]{3,2,1,0:T(8,128)S(1)}, f32[1,8,64,1024]{3,2,1,0:T(8,128)}, u32[]{:S(2)}) copy-start(f32[1,8,64,1024]{3,2,1,0:T(8,128)} %param.14) | copy-start | bytes 6291460
  36.2 7.5 %dynamic-slice-start = ((f32[2048]{0:T(1024)}, s32[]{:T(128)}), f32[1024]{0:T(1024)S(1)}, s32[]{:S(2)}) async-start(f32[2048]{0:T(1024)} %param.13, s32[]{:T(128)} %select_n.52), calls=%async_computation.15 | async-start | bytes 8704 | tf_op jit(solution)/shard_map/dynamic_slice | solution.py:29
  36.2 112.0 %all-to-all-start.2 = ((bf16[8,2,1,144,1024]{4,3,1,2,0:T(8,128)(2,1)}), bf16[8,2,1,144,1024]{4,3,1,2,0:T(8,128)(2,1)}, u32[]{:S(2)}, u32[]{:S(2)}) async-start(bf16[8,2,1,144,1024]{4,3,1,2,0:T(8,128)(2,1)} %dynamic-slice_bitcast_fusion), calls=%async_computation.2 | async-start | bytes 9437184 | tf_op jit(solution)/shard_map/all_to_all | solution.py:80
  43.6 15.7 %all-gather.13.cloned.1.call-start = ((), (), s32[]{:S(2)}) async-start(), calls=%async_computation.9 | async-start | bytes 3145728 | tf_op jit(solution)/shard_map/all_gather | solution.py:40
  47.2 1.6 copy-start.6
  47.2 110.4 %all-gather.9.cloned.1.call-start = ((), (), s32[]{:S(2)}) async-start(), calls=%async_computation.7 | async-start | bytes 3145728 | tf_op jit(solution)/shard_map/all_gather | solution.py:39
  48.0 256.2 %all-gather.17.cloned.1.call-start = ((), (), s32[]{:S(2)}) async-start(), calls=%async_computation.11 | async-start | bytes 3145728 | tf_op jit(solution)/shard_map/all_gather | solution.py:41
  148.2 52.1 %all-to-all-start.3 = ((bf16[2,8,64,1024]{3,2,0,1:T(8,128)(2,1)}), bf16[2,8,64,1024]{3,2,0,1:T(8,128)(2,1)S(1)}, u32[]{:S(2)}, u32[]{:S(2)}) async-start(bf16[2,8,64,1024]{3,2,0,1:T(8,128)(2,1)} %copy.63), calls=%async_computation.3 | async-start | bytes 4194304 | tf_op jit(solution)/shard_map/all_to_all | solution.py:45
  151.8 194.8 %all-gather.11.cloned.1.call-start = ((), (), s32[]{:S(2)}) async-start(), calls=%async_computation.8 | async-start | bytes 14155776 | tf_op jit(solution)/shard_map/all_gather | solution.py:81
  200.2 52.2 %all-to-all-start = ((bf16[2,8,64,1024]{3,2,0,1:T(8,128)(2,1)}), bf16[2,8,64,1024]{3,2,0,1:T(8,128)(2,1)}, u32[]{:S(2)}, u32[]{:S(2)}) async-start(bf16[2,8,64,1024]{3,2,0,1:T(8,128)(2,1)} %copy.53), calls=%async_computation | async-start | bytes 4194304 | tf_op jit(solution)/shard_map/all_to_all | solution.py:44
  252.4 46.9 %all-to-all-start.4 = ((bf16[2,1,512,1024]{3,0,1,2:T(2,128)(2,1)}), bf16[2,1,512,1024]{3,0,1,2:T(2,128)(2,1)S(1)}, u32[]{:S(2)}, u32[]{:S(2)}) async-start(bf16[2,1,512,1024]{3,0,1,2:T(2,128)(2,1)} %copy.65), calls=%async_computation.4 | async-start | bytes 4194304 | tf_op jit(solution)/shard_map/all_to_all | solution.py:50
  299.3 4.9 copy-start.1
  299.3 29.5 %all-to-all-start.1 = ((bf16[2,1,512,1024]{3,0,1,2:T(2,128)(2,1)}), bf16[2,1,512,1024]{3,0,1,2:T(2,128)(2,1)}, u32[]{:S(2)}, u32[]{:S(2)}) async-start(bf16[2,1,512,1024]{3,0,1,2:T(2,128)(2,1)} %copy.55), calls=%async_computation.1 | async-start | bytes 4194304 | tf_op jit(solution)/shard_map/all_to_all | solution.py:49
  328.8 53.6 %all-to-all-start.5 = ((bf16[2,8,64,1024]{3,2,0,1:T(8,128)(2,1)}), bf16[2,8,64,1024]{3,2,0,1:T(8,128)(2,1)}, u32[]{:S(2)}, u32[]{:S(2)}) async-start(bf16[2,8,64,1024]{3,2,0,1:T(8,128)(2,1)} %copy.68), calls=%async_computation.5 | async-start | bytes 4194304 | tf_op jit(solution)/shard_map/all_to_all | solution.py:46
  334.9 60.1 %all-gather.15.cloned.1.call-start = ((), (), s32[]{:S(2)}) async-start(), calls=%async_computation.10 | async-start | bytes 3538944 | tf_op jit(solution)/shard_map/all_gather | solution.py:85
  337.3 1.3 copy-start
  346.6 6.0 copy-start.7
  346.6 7.6 %copy-start.14 = (bf16[8,2,1,144,2048]{4,3,0,1,2:T(8,128)(2,1)S(1)}, bf16[8,2,1,144,2048]{4,3,0,1,2:T(8,128)(2,1)}, u32[]{:S(2)}) copy-start(bf16[8,2,1,144,2048]{4,3,0,1,2:T(8,128)(2,1)} %all-gather.11.cloned.1.call-done) | copy-start | bytes 28311556
  402.6 5.7 copy-start.12
  402.6 5.8 copy-start.11
  402.6 8.2 %copy-start.10 = (f32[64,1024]{1,0:T(8,128)S(1)}, f32[64,1024]{1,0:T(8,128)}, u32[]{:S(2)}) copy-start(f32[64,1024]{1,0:T(8,128)} %param.19) | copy-start | bytes 786436
  402.6 8.9 %copy-start.13 = (f32[192,8]{0,1:T(8,128)S(1)}, f32[192,8]{0,1:T(8,128)}, u32[]{:S(2)}) copy-start(f32[192,8]{0,1:T(8,128)} %param.12) | copy-start | bytes 18436
  402.6 225.5 %all-to-all-start.6 = ((bf16[8,2,1,144,1024]{4,3,1,2,0:T(8,128)(2,1)}), bf16[8,2,1,144,1024]{4,3,1,2,0:T(8,128)(2,1)}, u32[]{:S(2)}, u32[]{:S(2)}) async-start(bf16[8,2,1,144,1024]{4,3,1,2,0:T(8,128)(2,1)} %copy.70), calls=%async_computation.6 | async-start | bytes 9437184 | tf_op jit(solution)/shard_map/all_to_all | solution.py:89
  408.3 117.5 %all-gather.19.cloned.1.call-start = ((), (), s32[]{:S(2)}) async-start(), calls=%async_computation.12 | async-start | bytes 1179648 | tf_op jit(solution)/shard_map/all_gather | solution.py:53
  410.2 154.7 %all-gather.21.cloned.1.call-start = ((), (), s32[]{:S(2)}) async-start(), calls=%async_computation.13 | async-start | bytes 1179648 | tf_op jit(solution)/shard_map/all_gather | solution.py:54
  410.8 195.7 %all-gather.23.cloned.1.call-start = ((), (), s32[]{:S(2)}) async-start(), calls=%async_computation.14 | async-start | bytes 1179648 | tf_op jit(solution)/shard_map/all_gather | solution.py:55
  621.7 4.1 copy-start.2
  638.2 1.2 copy-start.3
  638.2 2.4 copy-start.4
  639.5 2.1 copy-start.9
Sparse Core Ops, SparseCore 0:
  47.3 11.9 all-gather.12
  61.4 11.7 all-gather.8
  75.3 11.7 all-gather.16
  157.7 138.2 all-gather.10
  358.5 36.4 all-gather.14
Sparse Core Ops, SparseCore 1:
  411.5 114.3 all-gather.18
  528.4 36.5 all-gather.20
  567.5 38.9 all-gather.22
where the time goes:
time: 660 us; the launch traced here: 651 us
  waiting for transfers between devices  457 us (69%)
  local copies, waits for them, and re-layouts  101 us (15%)
  starting transfers between devices  36.7 us (6%)
  matrix products  20.4 us (3%)
  between operations  16 us (2%)
  other arithmetic  13.6 us (2%)
    all_gather x1, waiting for transfers between devices, on_device(): lax.all_gather(gate_sh_local, 'fs', axis=0, tiled=True)  114 us
    all_to_all x1, waiting for transfers between devices, on_device(): lax.all_to_all(send, 'fs', split_axis=0, concat_axis=0, tiled=True)  85.7 us
    all_to_all x1, waiting for transfers between devices, on_device(): lax.all_to_all(halves[0], 'fs', split_axis=1, concat_axis=2, tiled=True)  44.2 us
    all_gather x1, waiting for transfers between devices, on_device(): lax.all_gather(down_sh_local, 'fs', axis=0, tiled=True)  41.5 us
    all_to_all x1, waiting for transfers between devices, on_device(): lax.all_to_all(halves[1], 'fs', split_axis=1, concat_axis=2, tiled=True)  39.5 us
    all_gather x1, waiting for transfers between devices, on_device(): lax.all_gather(up_sh_local, 'fs', axis=0, tiled=True)  39.1 us
    all_to_all x1, waiting for transfers between devices, on_device(): lax.all_to_all(up_cols, 'tp', split_axis=2, concat_axis=3, tiled=True)  37.9 us
    all_to_all x1, waiting for transfers between devices, on_device(): lax.all_to_all(halves[2], 'fs', split_axis=1, concat_axis=2, tiled=True)  24 us
  transfers between devices with their start and end apart: 15, of which 11 were waited for; matrix products, arithmetic and copies ran while one was open for 12% of the time, Pallas kernels for 0%

commit v1 on v0

--- a/solution.py
+++ b/solution.py
@@ -42,7 +42,12 @@
     )
     gate_cols, up_cols, down_w = (
         lax.all_to_all(halves[0], "fs", split_axis=1, concat_axis=2, tiled=True),
-        lax.all_to_all(halves[1], "fs", split_axis=1, concat_axis=2, tiled=True),
+        jnp.concatenate(
+            lax.all_to_all(
+                jnp.stack(jnp.split(halves[1], lax.axis_size("fs"), axis=1)), "fs", 0, 0
+            ),
+            axis=2,
+        ),
         lax.all_to_all(halves[2], "fs", split_axis=1, concat_axis=2, tiled=True),
     )
     gate_w, up_w = (

time: 660 us -> 662 us (level)
    unnamed x37 -> x48, local copies, waits for them, and re-layouts: 14.4 us -> 23.7 us
where the time goes in v1:
time: 662 us; the launch traced here: 652 us
  waiting for transfers between devices  456 us (69%)
  local copies, waits for them, and re-layouts  104 us (16%)
  starting transfers between devices  36.8 us (6%)
  matrix products  20.4 us (3%)
  between operations  16 us (2%)
  other arithmetic  13.6 us (2%)
    all_gather x1, waiting for transfers between devices, on_device(): lax.all_gather(gate_sh_local, 'fs', axis=0, tiled=True)  114 us
    all_to_all x1, waiting for transfers between devices, on_device(): lax.all_to_all(send, 'fs', split_axis=0, concat_axis=0, tiled=True)  79.8 us
    all_to_all x1, waiting for transfers between devices, on_device(): lax.all_to_all(halves[0], 'fs', split_axis=1, concat_axis=2, tiled=True)  43.9 us
    all_to_all x1, waiting for transfers between devices, on_device(): lax.all_to_all(jnp.stack(jnp.split(halves[1], lax.axis_size('fs'), axis=1...  43.1 us
    all_gather x1, waiting for transfers between devices, on_device(): lax.all_gather(down_sh_local, 'fs', axis=0, tiled=True)  41.5 us
    all_gather x1, waiting for transfers between devices, on_device(): lax.all_gather(up_sh_local, 'fs', axis=0, tiled=True)  39.1 us
    all_to_all x1, waiting for transfers between devices, on_device(): lax.all_to_all(up_cols, 'tp', split_axis=2, concat_axis=3, tiled=True)  37.3 us
    all_to_all x1, waiting for transfers between devices, on_device(): lax.all_to_all(halves[2], 'fs', split_axis=1, concat_axis=2, tiled=True)  24 us
  transfers between devices with their start and end apart: 15, of which 11 were waited for; matrix products, arithmetic and copies ran while one was open for 12% of the time, Pallas kernels for 0%

profile of v1, /device:TPU:0, one launch (start us, length us, event | category | flops | bytes accessed | tf_op | source)
XLA Modules:
  0.0 651.9 jit_solution(541479395586688135)
XLA Ops:
  9.2 4.5 reduce-window.6
  14.6 1.4 fusion.23
  16.2 14.7 %scatter_custom_fusion = bf16[2304,2048]{1,0:T(8,128)(2,1)} fusion(s32[1536]{0:T(1024)S(1)} %fusion.38, bf16[]{:T(256)} %constant.72.clone.1, bf16[192,2048]{1,0:T(8,128)(2,1)S(1)} %fusion.24), kind=kCustom, calls=%fused_computation.6 | custom fusion | bytes 10223618 | tf_op jit(solution)/shard_map/scatter | solution.py:81
  30.9 5.2 dynamic-slice_bitcast_fusion
  36.2 7.4 %all-to-all-start.2 = ((bf16[8,2,1,144,1024]{4,3,1,2,0:T(8,128)(2,1)}), bf16[8,2,1,144,1024]{4,3,1,2,0:T(8,128)(2,1)}, u32[]{:S(2)}, u32[]{:S(2)}) async-start(bf16[8,2,1,144,1024]{4,3,1,2,0:T(8,128)(2,1)} %dynamic-slice_bitcast_fusion), calls=%async_computation.2 | async-start | bytes 9437184 | tf_op jit(solution)/shard_map/all_to_all | solution.py:85
  43.7 3.5 fusion.18
  48.8 1.1 convert_element_type.57
  49.9 9.4 %all-gather.13.cloned.1.call-done = bf16[2,8,64,1024]{3,2,0,1:T(8,128)(2,1)} async-done(((bf16[1,8,64,1024]{3,2,0,1:T(8,128)(2,1)}), bf16[2,8,64,1024]{3,2,0,1:T(8,128)(2,1)}) %all-gather.13.cloned.1.call-update) | async-done | bytes 2097168 | tf_op jit(solution)/shard_map/all_gather | solution.py:40
  59.3 1.0 fusion.34
  60.3 1.0 fusion.33
  61.2 1.0 fusion.32
  62.2 1.0 fusion.31
  63.2 1.0 fusion.30
  64.1 1.0 fusion.29
  65.1 1.0 fusion.28
  66.1 1.0 fusion.27
  67.1 1.3 copy-done.7
  68.4 79.8 %all-to-all-done.2 = bf16[8,2,1,144,1024]{4,3,1,2,0:T(8,128)(2,1)} async-done(((bf16[8,2,1,144,1024]{4,3,1,2,0:T(8,128)(2,1)}), bf16[8,2,1,144,1024]{4,3,1,2,0:T(8,128)(2,1)}, u32[]{:S(2)}, u32[]{:S(2)}) %all-to-all-start.2) | async-done | bytes 4718624 | tf_op jit(solution)/shard_map/all_to_all | solution.py:85
  148.1 3.6 all-to-all-start.3
  151.8 5.2 copy.91
  157.1 43.1 %all-to-all-done.3 = bf16[8,2,1,64,1024]{4,3,1,2,0:T(8,128)(2,1)S(1)} async-done(((bf16[8,2,1,64,1024]{4,3,1,2,0:T(8,128)(2,1)}), bf16[8,2,1,64,1024]{4,3,1,2,0:T(8,128)(2,1)S(1)}, u32[]{:S(2)}, u32[]{:S(2)}) %all-to-all-start.3) | async-done | bytes 2097184 | tf_op jit(solution)/shard_map/all_to_all | solution.py:46
  200.2 4.8 all-to-all-start
  205.2 3.5 copy.94
  208.7 43.9 %all-to-all-done = bf16[2,8,64,1024]{3,2,0,1:T(8,128)(2,1)} async-done(((bf16[2,8,64,1024]{3,2,0,1:T(8,128)(2,1)}), bf16[2,8,64,1024]{3,2,0,1:T(8,128)(2,1)}, u32[]{:S(2)}, u32[]{:S(2)}) %all-to-all-start) | async-done | bytes 2097184 | tf_op jit(solution)/shard_map/all_to_all | solution.py:44
  252.6 3.8 all-to-all-start.4
  256.4 5.1 copy.84
  261.5 37.3 %all-to-all-done.4 = bf16[2,1,512,1024]{3,0,1,2:T(2,128)(2,1)S(1)} async-done(((bf16[2,1,512,1024]{3,0,1,2:T(2,128)(2,1)}), bf16[2,1,512,1024]{3,0,1,2:T(2,128)(2,1)S(1)}, u32[]{:S(2)}, u32[]{:S(2)}) %all-to-all-start.4) | async-done | bytes 2097184 | tf_op jit(solution)/shard_map/all_to_all | solution.py:55
  298.8 1.3 copy-done.1
  300.1 4.8 all-to-all-start.1
  305.0 3.3 copy.97
  308.9 3.5 copy.96
  312.4 4.5 reshape.250
  316.9 12.7 %all-to-all-done.1 = bf16[2,1,512,1024]{3,0,1,2:T(2,128)(2,1)} async-done(((bf16[2,1,512,1024]{3,0,1,2:T(2,128)(2,1)}), bf16[2,1,512,1024]{3,0,1,2:T(2,128)(2,1)}, u32[]{:S(2)}, u32[]{:S(2)}) %all-to-all-start.1) | async-done | bytes 2097184 | tf_op jit(solution)/shard_map/all_to_all | solution.py:54
  329.5 6.2 all-to-all-start.5
  335.9 2.2 copy.85
  338.1 1.3 copy-done
  339.4 3.5 copy.86
  342.9 4.5 reshape.249
  347.4 6.0 fusion
  353.4 1.6 copy-done.16
  355.0 4.1 fusion.10
  359.2 24.0 %all-to-all-done.5 = bf16[2,8,64,1024]{3,2,0,1:T(8,128)(2,1)} async-done(((bf16[2,8,64,1024]{3,2,0,1:T(8,128)(2,1)}), bf16[2,8,64,1024]{3,2,0,1:T(8,128)(2,1)}, u32[]{:S(2)}, u32[]{:S(2)}) %all-to-all-start.5) | async-done | bytes 2097184 | tf_op jit(solution)/shard_map/all_to_all | solution.py:51
  383.2 3.1 copy.98
  386.3 9.4 %all-gather.15.cloned.1.call-done = bf16[8,2,1,144,512]{4,3,0,1,2:T(8,128)(2,1)} async-done(((bf16[8,2,1,144,256]{4,3,0,1,2:T(8,128)(2,1)}), bf16[8,2,1,144,512]{4,3,0,1,2:T(8,128)(2,1)}) %all-gather.15.cloned.1.call-update) | async-done | bytes 2359312 | tf_op jit(solution)/shard_map/all_gather | solution.py:90
  395.8 4.9 convert_bitcast_fusion
  400.7 2.7 copy.99
  403.4 5.7 all-to-all-start.6
  409.2 1.8 multiply_convert_fusion.1
  412.5 114.1 %all-gather.19.cloned.1.call-done = bf16[2048,256]{1,0:T(8,128)(2,1)} async-done(((bf16[256,256]{1,0:T(8,128)(2,1)}), bf16[2048,256]{1,0:T(8,128)(2,1)}) %all-gather.19.cloned.1.call-update) | async-done | bytes 1048592 | tf_op jit(solution)/shard_map/all_gather | solution.py:58
  526.6 39.1 %all-gather.21.cloned.1.call-done = bf16[2048,256]{1,0:T(8,128)(2,1)} async-done(((bf16[256,256]{1,0:T(8,128)(2,1)}), bf16[2048,256]{1,0:T(8,128)(2,1)}) %all-gather.21.cloned.1.call-update) | async-done | bytes 1048592 | tf_op jit(solution)/shard_map/all_gather | solution.py:59
  565.8 41.5 %all-gather.23.cloned.1.call-done = bf16[512,1024]{1,0:T(8,128)(2,1)} async-done(((bf16[64,1024]{1,0:T(8,128)(2,1)}), bf16[512,1024]{1,0:T(8,128)(2,1)}) %all-gather.23.cloned.1.call-update) | async-done | bytes 1048592 | tf_op jit(solution)/shard_map/all_gather | solution.py:60
  607.3 1.6 fusion.41
  608.9 1.6 fusion.26
  610.5 5.5 all_gather.34
  616.0 2.5 copy.101
  618.5 4.1 copy.100
  622.6 2.4 copy.104
  625.0 3.9 copy.103
  628.9 10.0 %gather_fusion = bf16[1536,1024]{1,0:T(8,128)(2,1)S(1)} fusion(bf16[2304,1024]{1,0:T(8,128)(2,1)} %bitcast.36, s32[2048]{0:T(1024)S(1)} %pad_clamp_fusion), kind=kCustom, calls=%fused_computation | custom fusion | bytes 6297600 | tf_op jit(solution)/shard_map/gather | solution.py:95
  639.0 1.0 fusion.7
  640.2 1.1 fusion.25
  641.4 1.0 copy.124
  642.4 1.0 copy.125
  643.4 1.0 copy.126
  (71 shorter events, 6.9 us)
Async XLA Ops:
  8.0 8.0 %copy-start.6 = (bf16[192,2048]{1,0:T(8,128)(2,1)S(1)}, bf16[192,2048]{1,0:T(8,128)(2,1)}, u32[]{:S(2)}) copy-start(bf16[192,2048]{1,0:T(8,128)(2,1)} %param.10) | copy-start | bytes 2359300
  36.2 7.5 %copy-start.10 = (f32[1,8,64,1024]{3,2,1,0:T(8,128)S(1)}, f32[1,8,64,1024]{3,2,1,0:T(8,128)}, u32[]{:S(2)}) copy-start(f32[1,8,64,1024]{3,2,1,0:T(8,128)} %param.14) | copy-start | bytes 6291460
  36.2 7.5 %dynamic-slice-start = ((f32[2048]{0:T(1024)}, s32[]{:T(128)}), f32[1024]{0:T(1024)S(1)}, s32[]{:S(2)}) async-start(f32[2048]{0:T(1024)} %param.13, s32[]{:T(128)} %select_n.52), calls=%async_computation.15 | async-start | bytes 8704 | tf_op jit(solution)/shard_map/dynamic_slice | solution.py:29
  36.2 112.0 %all-to-all-start.2 = ((bf16[8,2,1,144,1024]{4,3,1,2,0:T(8,128)(2,1)}), bf16[8,2,1,144,1024]{4,3,1,2,0:T(8,128)(2,1)}, u32[]{:S(2)}, u32[]{:S(2)}) async-start(bf16[8,2,1,144,1024]{4,3,1,2,0:T(8,128)(2,1)} %dynamic-slice_bitcast_fusion), calls=%async_computation.2 | async-start | bytes 9437184 | tf_op jit(solution)/shard_map/all_to_all | solution.py:85
  43.6 15.7 %all-gather.13.cloned.1.call-start = ((), (), s32[]{:S(2)}) async-start(), calls=%async_computation.9 | async-start | bytes 3145728 | tf_op jit(solution)/shard_map/all_gather | solution.py:40
  47.2 1.6 copy-start.8
  47.2 109.9 %all-gather.9.cloned.1.call-start = ((), (), s32[]{:S(2)}) async-start(), calls=%async_computation.7 | async-start | bytes 3145728 | tf_op jit(solution)/shard_map/all_gather | solution.py:39
  47.9 257.0 %all-gather.17.cloned.1.call-start = ((), (), s32[]{:S(2)}) async-start(), calls=%async_computation.11 | async-start | bytes 3145728 | tf_op jit(solution)/shard_map/all_gather | solution.py:41
  67.1 1.3 copy-start.7
  148.1 52.1 %all-to-all-start.3 = ((bf16[8,2,1,64,1024]{4,3,1,2,0:T(8,128)(2,1)}), bf16[8,2,1,64,1024]{4,3,1,2,0:T(8,128)(2,1)S(1)}, u32[]{:S(2)}, u32[]{:S(2)}) async-start(bf16[8,2,1,64,1024]{4,3,1,2,0:T(8,128)(2,1)} %copy-done.7), calls=%async_computation.3 | async-start | bytes 4194304 | tf_op jit(solution)/shard_map/all_to_all | solution.py:46
  151.8 195.6 %all-gather.11.cloned.1.call-start = ((), (), s32[]{:S(2)}) async-start(), calls=%async_computation.8 | async-start | bytes 14155776 | tf_op jit(solution)/shard_map/all_gather | solution.py:86
  200.2 52.4 %all-to-all-start = ((bf16[2,8,64,1024]{3,2,0,1:T(8,128)(2,1)}), bf16[2,8,64,1024]{3,2,0,1:T(8,128)(2,1)}, u32[]{:S(2)}, u32[]{:S(2)}) async-start(bf16[2,8,64,1024]{3,2,0,1:T(8,128)(2,1)} %all-gather.9.cloned.1.call-done), calls=%async_computation | async-start | bytes 4194304 | tf_op jit(solution)/shard_map/all_to_all | solution.py:44
  252.6 46.2 %all-to-all-start.4 = ((bf16[2,1,512,1024]{3,0,1,2:T(2,128)(2,1)}), bf16[2,1,512,1024]{3,0,1,2:T(2,128)(2,1)S(1)}, u32[]{:S(2)}, u32[]{:S(2)}) async-start(bf16[2,1,512,1024]{3,0,1,2:T(2,128)(2,1)} %copy.94), calls=%async_computation.4 | async-start | bytes 4194304 | tf_op jit(solution)/shard_map/all_to_all | solution.py:55
  298.8 1.3 copy-start.1
  300.1 29.4 %all-to-all-start.1 = ((bf16[2,1,512,1024]{3,0,1,2:T(2,128)(2,1)}), bf16[2,1,512,1024]{3,0,1,2:T(2,128)(2,1)}, u32[]{:S(2)}, u32[]{:S(2)}) async-start(bf16[2,1,512,1024]{3,0,1,2:T(2,128)(2,1)} %bitcast.149), calls=%async_computation.1 | async-start | bytes 4194304 | tf_op jit(solution)/shard_map/all_to_all | solution.py:54
  305.0 3.3 copy-start.2
  329.5 53.6 %all-to-all-start.5 = ((bf16[2,8,64,1024]{3,2,0,1:T(8,128)(2,1)}), bf16[2,8,64,1024]{3,2,0,1:T(8,128)(2,1)}, u32[]{:S(2)}, u32[]{:S(2)}) async-start(bf16[2,8,64,1024]{3,2,0,1:T(8,128)(2,1)} %copy.97), calls=%async_computation.5 | async-start | bytes 4194304 | tf_op jit(solution)/shard_map/all_to_all | solution.py:51
  335.7 60.1 %all-gather.15.cloned.1.call-start = ((), (), s32[]{:S(2)}) async-start(), calls=%async_computation.10 | async-start | bytes 3538944 | tf_op jit(solution)/shard_map/all_gather | solution.py:90
  338.1 1.3 copy-start
  347.4 6.0 copy-start.9
  347.4 7.6 %copy-start.16 = (bf16[8,2,1,144,2048]{4,3,0,1,2:T(8,128)(2,1)S(1)}, bf16[8,2,1,144,2048]{4,3,0,1,2:T(8,128)(2,1)}, u32[]{:S(2)}) copy-start(bf16[8,2,1,144,2048]{4,3,0,1,2:T(8,128)(2,1)} %all-gather.11.cloned.1.call-done) | copy-start | bytes 28311556
  403.4 5.7 copy-start.14
  403.4 5.8 copy-start.13
  403.4 8.2 %copy-start.12 = (f32[64,1024]{1,0:T(8,128)S(1)}, f32[64,1024]{1,0:T(8,128)}, u32[]{:S(2)}) copy-start(f32[64,1024]{1,0:T(8,128)} %param.19) | copy-start | bytes 786436
  403.4 8.9 %copy-start.15 = (f32[192,8]{0,1:T(8,128)S(1)}, f32[192,8]{0,1:T(8,128)}, u32[]{:S(2)}) copy-start(f32[192,8]{0,1:T(8,128)} %param.12) | copy-start | bytes 18436
  403.4 225.5 %all-to-all-start.6 = ((bf16[8,2,1,144,1024]{4,3,1,2,0:T(8,128)(2,1)}), bf16[8,2,1,144,1024]{4,3,1,2,0:T(8,128)(2,1)}, u32[]{:S(2)}, u32[]{:S(2)}) async-start(bf16[8,2,1,144,1024]{4,3,1,2,0:T(8,128)(2,1)} %copy.99), calls=%async_computation.6 | async-start | bytes 9437184 | tf_op jit(solution)/shard_map/all_to_all | solution.py:94
  409.1 117.5 %all-gather.19.cloned.1.call-start = ((), (), s32[]{:S(2)}) async-start(), calls=%async_computation.12 | async-start | bytes 1179648 | tf_op jit(solution)/shard_map/all_gather | solution.py:58
  411.0 154.7 %all-gather.21.cloned.1.call-start = ((), (), s32[]{:S(2)}) async-start(), calls=%async_computation.13 | async-start | bytes 1179648 | tf_op jit(solution)/shard_map/all_gather | solution.py:59
  411.6 195.7 %all-gather.23.cloned.1.call-start = ((), (), s32[]{:S(2)}) async-start(), calls=%async_computation.14 | async-start | bytes 1179648 | tf_op jit(solution)/shard_map/all_gather | solution.py:60
  618.5 4.1 copy-start.3
  639.0 1.2 copy-start.4
  640.2 1.2 copy-start.5
  640.2 2.2 copy-start.11
Sparse Core Ops, SparseCore 0:
  47.3 11.9 all-gather.12
  61.4 11.7 all-gather.8
  75.3 11.7 all-gather.16
  157.2 137.6 all-gather.10
  359.3 36.4 all-gather.14
Sparse Core Ops, SparseCore 1:
  412.3 114.3 all-gather.18
  529.2 36.5 all-gather.20
  568.3 38.9 all-gather.22
